TPU v7x, 32 devices: a whole 2x2x4 slice. The times are simulated.
32 devices in a mesh: sp: 8 (over z, y), tp: 4 (over x, core).
Axes of the slice: x: 2, y: 2, z: 4, core: 2. Of those that a mesh axis runs over, the one named last changes fastest.
Arguments:
- inputs: bfloat16 [2, 1024, 2048], P(None, 'sp'), may hold values from -6 to 6
- norm_gain: float32 [2048], replicated, may hold values from 0.1 to 1.9
- query_weight: bfloat16 [2048, 1024], P('sp', 'tp'), may hold values from -0.125 to 0.125
- key_weight: bfloat16 [2048, 256], P('sp', 'tp'), may hold values from -0.125 to 0.125
- value_weight: bfloat16 [2048, 256], P('sp', 'tp'), may hold values from -0.125 to 0.125
- query_gain: float32 [64], replicated, may hold values from 0.1 to 24
- key_gain: float32 [64], replicated, may hold values from 0.1 to 1.9
- forget_cache: float32 [2, 16, 1024], P(None, 'tp'), may hold values from -104 to 0, as said below
- rec_in_weight: bfloat16 [2048, 1024], P('sp', 'tp'), may hold values from -0.125 to 0.125
- rec_gate_weight: bfloat16 [2048, 1024], P('sp', 'tp'), may hold values from -0.125 to 0.125
- conv_weight: bfloat16 [4, 1024], P(None, 'tp'), may hold values from -3 to 3
- decay_gate_weight: bfloat16 [16, 64, 64], P('tp'), may hold values from -0.75 to 0.75
- input_gate_weight: bfloat16 [16, 64, 64], P('tp'), may hold values from -0.75 to 0.75
- decay_param: float32 [1024], P('tp'), may hold values from 4 to 16
- decay_extra: float32 [2, 1024, 1024], P(None, 'sp', 'tp'), may hold values from -2 to 0
- attn_out_gain: float32 [1024], P('tp'), may hold values from 0.1 to 1.9
- rec_out_gain: float32 [1024], P('tp'), may hold values from 0.1 to 1.9
- out_att_weight: bfloat16 [1024, 2048], P('tp'), may hold values from -0.125 to 0.125
- out_rec_weight: bfloat16 [1024, 2048], P('tp'), may hold values from -0.125 to 0.125
Outputs:
- mixed: bfloat16 [2, 1024, 2048], P(None, 'sp', 'tp')
Inputs may be any that keep to these rules, and one draw needn't show every extreme that they name: `forget_cache`: Non-increasing along the positions of each sequence and head.
All inputs are finite; a program needn't handle non-finite values.
Results may differ from a plain program's by a relative error of at most 0.012.
The roundings to bfloat16 on the way count: a program that leaves them out, or rounds other values in their place, can miss the bound.
Values may be sent and summed in bfloat16 or wider, within the bound.
A program may use at most 128 MiB of HBM per device.

v0:
```python
import jax
import jax.numpy as jnp
from jax import lax
from jax.sharding import PartitionSpec as P

D = 2048
LRU_BLOCK = 64
CONV_TAPS = 4
lru_const = 8.0
norm_eps = 1e-06


def from_behind(value, axis, steps):
    count = lax.axis_size(axis)
    leading, last = (max(0, -steps), min(count, count - steps))
    return lax.ppermute(value, axis, [(source, source + steps) for source in range(leading, last)])


def rms_scale(values, gain):
    multiplier = lax.rsqrt(jnp.mean(values * values, axis=-1, keepdims=True) + norm_eps)
    return values * multiplier * gain


def merge_state(earlier, later):
    return (earlier[0] * later[0], later[0] * earlier[1] + later[1])


def block_length(length, span):
    shards = max(length // span, 1)
    group_size = 1
    for trial_size in range(1, shards + 1):
        if shards % trial_size == 0 and trial_size * span <= 1024:
            group_size = trial_size
    sub_size = group_size * span
    if length % sub_size:
        sub_size = length
    return sub_size


def body(
    inputs,
    norm_gain,
    query_weight,
    key_weight,
    value_weight,
    query_gain,
    key_gain,
    forget_cache,
    rec_in_weight,
    rec_gate_weight,
    conv_weight,
    decay_gate_weight,
    input_gate_weight,
    decay_param,
    decay_extra,
    attn_out_gain,
    rec_out_gain,
    out_att_weight,
    out_rec_weight,
):
    seq_count, seq_span, model_width = inputs.shape
    row_count = seq_count * seq_span
    head_dim = query_gain.shape[0]
    att_local = query_weight.shape[1] // head_dim
    kv_local = key_weight.shape[1] // head_dim
    head_group = att_local // kv_local
    channels = rec_in_weight.shape[1]
    normed = rms_scale(
        inputs.reshape(row_count, model_width).astype(jnp.float32), norm_gain
    ).astype(jnp.bfloat16)
    normed_cols = normed.T
    row_contract = (((0,), (0,)), ((), ()))
    kv_cols = key_weight.shape[1]
    pieces = (
        lax.all_gather(query_weight, "sp", axis=0, tiled=True),
        lax.all_gather(key_weight, "sp", axis=0, tiled=True),
        lax.all_gather(value_weight, "sp", axis=0, tiled=True),
        lax.all_gather(rec_in_weight, "sp", axis=0, tiled=True),
        lax.all_gather(rec_gate_weight, "sp", axis=0, tiled=True),
    )
    query_proj, key_proj, value_sum, rec_in_sum, gate_proj = tuple(
        (
            lax.dot_general(
                normed_cols, weight_part, row_contract, preferred_element_type=jnp.float32
            )
            for weight_part in pieces
        )
    )
    queries = rms_scale(query_proj.reshape(row_count, att_local, head_dim), query_gain).astype(
        jnp.bfloat16
    )
    queries = queries.reshape(seq_count, seq_span, kv_local, head_group, head_dim).transpose(
        0, 2, 3, 1, 4
    )
    queries = queries.reshape(seq_count, kv_local, head_group * seq_span, head_dim)
    key_heads = rms_scale(key_proj.reshape(row_count, kv_local, head_dim), key_gain).astype(
        jnp.bfloat16
    )
    key_heads = key_heads.reshape(seq_count, seq_span, kv_cols)
    value_heads = value_sum.astype(jnp.bfloat16).reshape(seq_count, seq_span, kv_cols)
    key_value = jnp.concatenate([key_heads, value_heads], axis=2)
    my_first = lax.axis_index("sp") * seq_span
    own_gates = lax.dynamic_slice_in_dim(forget_cache, my_first, seq_span, 2)
    own_gates = own_gates.reshape(seq_count, kv_local, head_group, seq_span, 1)
    query_pos = my_first + jnp.tile(jnp.arange(seq_span, dtype=jnp.int32), head_group)
    scaling = head_dim ** (-0.5)
    start_state = (
        jnp.full((seq_count, kv_local, head_group * seq_span), -jnp.inf, jnp.float32),
        jnp.zeros((seq_count, kv_local, head_group * seq_span), jnp.float32),
        jnp.zeros((seq_count, kv_local, head_group * seq_span, head_dim), jnp.float32),
    )
    shard_part = lax.all_gather(key_value, "sp", axis=1, tiled=True)
    offset = jnp.int32(0)
    length = shard_part.shape[1]
    sub_size = block_length(length, seq_span)

    def one_step(block_index, carried_state):
        key_first = offset + block_index * sub_size

        def work(carried):
            top_score, totals, accum = carried
            block_rows = lax.dynamic_slice_in_dim(shard_part, block_index * sub_size, sub_size, 1)
            key_block = block_rows[:, :, :kv_cols].reshape(seq_count, sub_size, kv_local, head_dim)
            value_block = block_rows[:, :, kv_cols:].reshape(
                seq_count, sub_size, kv_local, head_dim
            )
            key_gates = lax.dynamic_slice_in_dim(forget_cache, key_first, sub_size, 2)
            key_gates = key_gates.reshape(seq_count, kv_local, head_group, 1, sub_size)
            scores = (
                jnp.einsum(
                    "bhqd,bkhd->bhqk", queries, key_block, preferred_element_type=jnp.float32
                )
                * scaling
            )
            scores = (
                scores.reshape(seq_count, kv_local, head_group, seq_span, sub_size)
                + own_gates
                - key_gates
            )
            scores = scores.reshape(seq_count, kv_local, head_group * seq_span, sub_size)
            visible = (
                query_pos[:, None] >= (key_first + jnp.arange(sub_size, dtype=jnp.int32))[None, :]
            )
            scores = jnp.where(visible, scores, -jnp.inf)
            new_top = jnp.maximum(top_score, jnp.max(scores, axis=-1))
            safe_top = jnp.where(jnp.isfinite(new_top), new_top, 0.0)
            weights = jnp.exp(scores - safe_top[..., None])
            fading = jnp.exp(top_score - safe_top)
            totals = totals * fading + jnp.sum(weights, axis=-1)
            accum = accum * fading[..., None] + jnp.einsum(
                "bhqk,bkhd->bhqd",
                weights.astype(jnp.bfloat16),
                value_block,
                preferred_element_type=jnp.float32,
            )
            return (new_top, totals, accum)

        return lax.cond(
            key_first < my_first + seq_span, work, lambda carried: carried, carried_state
        )

    top_score, totals, accum = lax.fori_loop(0, length // sub_size, one_step, start_state)
    attended = (accum / totals[..., None]).reshape(
        seq_count, kv_local, head_group, seq_span, head_dim
    )
    attended = attended.transpose(0, 3, 1, 2, 4).reshape(row_count, att_local, head_dim)
    att_normed = rms_scale(attended, attn_out_gain.reshape(att_local, head_dim)).astype(
        jnp.bfloat16
    )
    att_normed = att_normed.reshape(row_count, att_local * head_dim)
    rec_in = rec_in_sum.astype(jnp.bfloat16).reshape(seq_count, seq_span, channels)
    before = from_behind(rec_in[:, seq_span - (CONV_TAPS - 1) :, :], "sp", 1)
    extended = jnp.concatenate([before, rec_in], axis=1)
    conv = jnp.zeros((seq_count, seq_span, channels), jnp.float32)
    for tap in range(CONV_TAPS):
        conv = conv + extended[:, tap : tap + seq_span].astype(jnp.float32) * conv_weight[
            tap
        ].astype(jnp.float32)
    conv = conv.astype(jnp.bfloat16)
    blocks_local = decay_gate_weight.shape[0]
    grouped = conv.reshape(seq_count, seq_span, blocks_local, LRU_BLOCK)
    gate_decay = jnp.einsum(
        "bsnd,nde->bsne", grouped, decay_gate_weight, preferred_element_type=jnp.float32
    ).reshape(seq_count, seq_span, channels)
    gate_input = jnp.einsum(
        "bsnd,nde->bsne", grouped, input_gate_weight, preferred_element_type=jnp.float32
    ).reshape(seq_count, seq_span, channels)
    log_decay = (
        -lru_const * jax.nn.sigmoid(gate_decay) * jax.nn.softplus(-decay_param) + decay_extra
    )
    drive = (
        jnp.sqrt(-jnp.expm1(2.0 * log_decay))
        * jax.nn.sigmoid(gate_input)
        * conv.astype(jnp.float32)
    )
    cum_decay, local_state = lax.associative_scan(merge_state, (jnp.exp(log_decay), drive), axis=1)
    every_decay, every_state = (
        lax.all_gather(cum_decay[:, seq_span - 1][None], "sp", axis=0, tiled=True),
        lax.all_gather(local_state[:, seq_span - 1][None], "sp", axis=0, tiled=True),
    )
    prefix_decay, prefix_state = lax.associative_scan(
        merge_state, (every_decay, every_state), axis=0
    )
    position = lax.axis_index("sp")
    earlier_state = lax.dynamic_index_in_dim(
        prefix_state, jnp.maximum(position - 1, 0), 0, keepdims=False
    )
    entering = jnp.where(position > 0, earlier_state, 0.0)
    state = local_state + cum_decay * entering[:, None, :]
    gated = state * jax.nn.gelu(gate_proj.reshape(seq_count, seq_span, channels))
    rec_normed = rms_scale(
        gated.reshape(row_count, blocks_local, LRU_BLOCK),
        rec_out_gain.reshape(blocks_local, LRU_BLOCK),
    ).astype(jnp.bfloat16)
    rec_normed = rec_normed.reshape(row_count, channels)
    out_cols = D // lax.axis_size("tp")
    pieces = row_count * lax.axis_size("tp") // row_count
    terms = jnp.dot(att_normed, out_att_weight, preferred_element_type=jnp.float32) + jnp.dot(
        rec_normed, out_rec_weight, preferred_element_type=jnp.float32
    )
    mixed_cols = lax.psum_scatter(
        terms.reshape(row_count, pieces, out_cols)
        .transpose(1, 0, 2)
        .reshape(pieces * row_count, out_cols)
        .astype(jnp.bfloat16),
        "tp",
        scatter_dimension=0,
        tiled=True,
    )
    return mixed_cols.reshape(seq_count, seq_span, out_cols)


def solution(mesh):
    return jax.shard_map(
        body,
        mesh=mesh,
        in_specs=(
            P(None, "sp", None),
            P(),
            P("sp", "tp"),
            P("sp", "tp"),
            P("sp", "tp"),
            P(),
            P(),
            P(None, "tp", None),
            P("sp", "tp"),
            P("sp", "tp"),
            P(None, "tp"),
            P("tp", None, None),
            P("tp", None, None),
            P("tp"),
            P(None, "sp", "tp"),
            P("tp"),
            P("tp"),
            P("tp", None),
            P("tp", None),
        ),
        out_specs=P(None, "sp", "tp"),
        check_vma=False,
    )
```

profile of v0, /device:TPU:0, one launch (start us, length us, event | category | flops | bytes accessed | tf_op | source)
XLA Modules:
  0.0 263.9 jit_solution(10849590766930557368)
XLA Ops:
  12.4 33.4 %all_gather.25 = bf16[2048,64]{0,1:T(8,128)(2,1)S(1)} all-gather(bf16[256,64]{0,1:T(8,128)(2,1)} %param.24), channel_id=1, replica_groups=mesh['sp'=8,'tp'=4] {'sp'}, dimensions={0}, use_global_device_ids=true | all-gather | bytes 294912 | tf_op jit(solution)/shard_map/all_gather | solution.py:76
  45.8 31.4 %all_gather.26 = bf16[2048,64]{0,1:T(8,128)(2,1)S(1)} all-gather(bf16[256,64]{0,1:T(8,128)(2,1)} %param.25), channel_id=1, replica_groups=mesh['sp'=8,'tp'=4] {'sp'}, dimensions={0}, use_global_device_ids=true | all-gather | bytes 294912 | tf_op jit(solution)/shard_map/all_gather | solution.py:77
  79.3 29.7 %all_gather.27 = bf16[2,1024,128]{1,2,0:T(8,128)(2,1)} all-gather(bf16[2,128,128]{1,2,0:T(8,128)(2,1)S(1)} %pad_maximum_fusion.3), channel_id=1, replica_groups=mesh['sp'=8,'tp'=4] {'sp'}, dimensions={1}, use_global_device_ids=true | all-gather | bytes 589824 | tf_op jit(solution)/shard_map/all_gather | solution.py:112
  110.3 2.4 copy.49
  112.6 1.7 multiply_reduce_fusion.1
  114.6 6.3 %conditional.1 = ((f32[2,1,512]{2,0,1:T(2,128)S(1)}, f32[2,1,512,64]{2,3,0,1:T(8,128)S(1)})) conditional(s32[]{:T(128)} %convert_element_type.124, (f32[2,1,512]{2,0,1:T(2,128)S(1)}, f32[2,1,512,64]{2,3,0,1:T(8,128)S(1)}) %tuple.30, (s32[]{:T(128)}, s32[4,128]{1,0:T(4,128)S(1)}, bf16[2,1,4,128,64]{3,2,4,0,1:T(4,128)(2,1)S(1)}, ...), branch_computations={%region_3.4_spmd, %region_4.7_spmd} | conditional | flops 281680384 | bytes 17967226 | solution.py:158
  115.9 2.4 fusion.3
  118.4 1.8 fusion.1
  121.5 1.7 convolution_convert_fusion
  123.3 3.3 %collective-permute-start = (bf16[2,3,256]{2,1,0:T(4,128)(2,1)S(1)}, bf16[2,3,256]{2,1,0:T(4,128)(2,1)S(1)}, u32[]{:S(2)}, u32[]{:S(2)}) collective-permute-start(bf16[2,3,256]{2,1,0:T(4,128)(2,1)S(1)} %slice.399), channel_id=1, source_target_pairs={{0,4},{4,8},{8,12},{12,16},{16,20},{20,24},{24,28},{1,5},{5,9},{9,... | collective-permute-start | bytes 9224 | tf_op jit(solution)/shard_map/ppermute | solution.py:16
  132.0 2.0 convert_multiply_fusion
  134.7 1.6 slice.363
  137.3 1.6 slice.316
  152.8 2.1 pad.116
  155.7 1.6 add.383
  157.3 1.7 fusion.45
  160.5 2.3 pad.118
  163.6 26.3 %all-gather = f32[16,1,256]{2,1,0:T(1,128)S(1)} all-gather(f32[2,1,256]{2,1,0:T(1,128)S(1)} %slice_add_fusion.4), channel_id=2, replica_groups=mesh['sp'=8,'tp'=4] {'sp'}, dimensions={0}, use_global_device_ids=true | all-gather | bytes 18432 | tf_op jit(solution)/shard_map/all_gather | solution.py:199
  190.4 1.6 pad_maximum_fusion.2
  197.7 26.1 %all-gather.1 = f32[16,1,256]{2,1,0:T(1,128)S(1)} all-gather(f32[2,1,256]{2,1,0:T(1,128)S(1)} %slice_add_fusion.3), channel_id=3, replica_groups=mesh['sp'=8,'tp'=4] {'sp'}, dimensions={0}, use_global_device_ids=true | all-gather | bytes 18432 | tf_op jit(solution)/shard_map/all_gather | solution.py:198
  224.9 3.0 %fusion.73 = (f32[2,128,256]{2,1,0:T(8,128)}, f32[2,128,256]{2,1,0:T(8,128)}) fusion(bf16[2,128,2048]{2,1,0:T(8,128)(2,1)} %multiply_convert_fusion, bf16[2048,256]{1,0:T(8,128)(2,1)} %all-gather.10.cloned.1.call-done, f32[2,256]{1,0:T(2,128)S(1)} %fusion.65, f32[2,128,256]{2,1,0:T(8,128)S(1)} %pad.131, f32[2,128,256]{2,1,0:T(8,128)} %pad.132, ...), kind=kOutput, calls=%fused_computation.170 | convolution fusion | flops 269352960 | bytes 3672064 | tf_op jit(solution)/shard_map/dot_general | solution.py:83
  227.9 1.8 copy.64
  232.1 1.7 fusion.12
  234.9 22.5 %reduce-scatter.2.cloned.1.call-done = bf16[256,512]{1,0:T(8,128)(2,1)} async-done(((bf16[1024,512]{1,0:T(8,128)(2,1)}), bf16[256,512]{1,0:T(8,128)(2,1)}) %reduce-scatter.2.cloned.1.call-update) | async-done | bytes 262160 | tf_op jit(solution)/shard_map/reduce_scatter | solution.py:221
  (216 shorter events, 46.3 us)
Async XLA Ops:
  6.5 120.2 %copy-start = (bf16[256,2048]{1,0:T(8,128)(2,1)S(1)}, bf16[256,2048]{1,0:T(8,128)(2,1)}, u32[]{:S(2)}) copy-start(bf16[256,2048]{1,0:T(8,128)(2,1)} %param.38) | copy-start | bytes 3145732
  6.5 70.7 %copy-start.1 = (bf16[2,128,2048]{2,1,0:T(8,128)(2,1)S(1)}, bf16[2,128,2048]{2,1,0:T(8,128)(2,1)}, u32[]{:S(2)}) copy-start(bf16[2,128,2048]{2,1,0:T(8,128)(2,1)} %param.21) | copy-start | bytes 3145732
  6.5 103.7 %all-gather.6.cloned.1.call-start = ((), (), s32[]{:S(2)}) async-start(), calls=%async_computation.1 | async-start | bytes 1179648 | tf_op jit(solution)/shard_map/all_gather | solution.py:75
  7.3 114.3 %all-gather.8.cloned.1.call-start = ((), (), s32[]{:S(2)}) async-start(), calls=%async_computation.2 | async-start | bytes 1179648 | tf_op jit(solution)/shard_map/all_gather | solution.py:78
  8.0 216.8 %all-gather.10.cloned.1.call-start = ((), (), s32[]{:S(2)}) async-start(), calls=%async_computation.3 | async-start | bytes 1179648 | tf_op jit(solution)/shard_map/all_gather | solution.py:79
  8.7 248.6 %reduce-scatter.2.cloned.1.call-start = ((), (), s32[]{:S(2)}) async-start(), calls=%async_computation.4 | async-start | bytes 1310720 | tf_op jit(solution)/shard_map/reduce_scatter | solution.py:221
  77.2 2.0 copy-start.15
  78.2 30.7 %copy-start.8 = (f32[2048]{0:T(1024)S(1)}, f32[2048]{0:T(1024)}, u32[]{:S(2)}) copy-start(f32[2048]{0:T(1024)} %param.22) | copy-start | bytes 24580
  110.2 2.4 copy-start.2
  112.6 1.7 copy-start.16
  115.9 2.5 copy-start.6
  118.3 1.8 copy-start.3
  121.0 5.6 %copy-start.13 = (f32[256]{0:T(256)S(1)}, f32[256]{0:T(256)}, u32[]{:S(2)}) copy-start(f32[256]{0:T(256)} %param.36) | copy-start | bytes 3076
  123.2 4.6 %copy-start.9 = (f32[1,256]{1,0:T(1,128)S(1)}, f32[1,256]{1,0:T(1,128)}, u32[]{:S(2)}) copy-start(f32[1,256]{1,0:T(1,128)} %get-tuple-element.199) | copy-start | bytes 3076
  123.2 4.6 %copy-start.10 = (f32[1,256]{1,0:T(1,128)S(1)}, f32[1,256]{1,0:T(1,128)}, u32[]{:S(2)}) copy-start(f32[1,256]{1,0:T(1,128)} %get-tuple-element.200) | copy-start | bytes 3076
  123.2 4.6 %copy-start.11 = (f32[1,256]{1,0:T(1,128)S(1)}, f32[1,256]{1,0:T(1,128)}, u32[]{:S(2)}) copy-start(f32[1,256]{1,0:T(1,128)} %get-tuple-element.201) | copy-start | bytes 3076
  123.2 4.6 %copy-start.12 = (f32[1,256]{1,0:T(1,128)S(1)}, f32[1,256]{1,0:T(1,128)}, u32[]{:S(2)}) copy-start(f32[1,256]{1,0:T(1,128)} %get-tuple-element.202) | copy-start | bytes 3076
  123.3 4.6 %collective-permute-start = (bf16[2,3,256]{2,1,0:T(4,128)(2,1)S(1)}, bf16[2,3,256]{2,1,0:T(4,128)(2,1)S(1)}, u32[]{:S(2)}, u32[]{:S(2)}) collective-permute-start(bf16[2,3,256]{2,1,0:T(4,128)(2,1)S(1)} %slice.399), channel_id=1, source_target_pairs={{0,4},{4,8},{8,12},{12,16},{16,20},{20,24},{24,28},{1,5},{5,9},{9,... | collective-permute-start | bytes 9224 | tf_op jit(solution)/shard_map/ppermute | solution.py:16
  126.6 2.2 copy-start.17
  128.1 0.7 copy-start.7
  144.1 7.1 %copy-start.4 = (f32[2,31,256]{2,1,0:T(8,128)S(1)}, f32[2,31,256]{2,1,0:T(8,128)}, u32[]{:S(2)}) copy-start(f32[2,31,256]{2,1,0:T(8,128)} %slice.361) | copy-start | bytes 190468
  144.2 7.1 %copy-start.5 = (f32[2,31,256]{2,1,0:T(8,128)S(1)}, f32[2,31,256]{2,1,0:T(8,128)}, u32[]{:S(2)}) copy-start(f32[2,31,256]{2,1,0:T(8,128)} %slice.320) | copy-start | bytes 190468
  224.8 7.1 %copy-start.14 = (f32[256]{0:T(256)S(1)}, f32[256]{0:T(256)}, u32[]{:S(2)}) copy-start(f32[256]{0:T(256)} %param.37) | copy-start | bytes 3076
Sparse Core Ops, SparseCore 0:
  9.5 44.2 all-gather.5
  55.9 41.5 all-gather.7
  99.6 38.9 all-gather.9
  235.0 22.3 reduce-scatter.1
where the time goes:
time: 265 us; the launch traced here: 264 us
  blocking collectives  147 us (55%)
  local copies, waits for them, and re-layouts  35.4 us (13%)
  waiting for transfers between devices  25.4 us (10%)
  other arithmetic  24.8 us (9%)
  matrix products  14.1 us (5%)
  between operations  13.9 us (5%)
  starting transfers between devices  3.38 us (1%)
    all_gather x1, blocking collectives, body(): lax.all_gather(key_weight, 'sp', axis=0, tiled=True)  33.4 us
    all_gather x1, blocking collectives, body(): lax.all_gather(value_weight, 'sp', axis=0, tiled=True)  31.4 us
    all_gather x1, blocking collectives, body(): shard_part = lax.all_gather(key_value, 'sp', axis=1, tiled=True)  29.7 us
    all_gather x1, blocking collectives, body(): lax.all_gather(local_state[:, seq_span - 1][None], 'sp', axis=0, tiled=True)  26.3 us
    all_gather x1, blocking collectives, body(): lax.all_gather(cum_decay[:, seq_span - 1][None], 'sp', axis=0, tiled=True)  26.1 us
    reduce_scatter x1, waiting for transfers between devices, body(): lax.psum_scatter(terms.reshape(row_count, pieces, out_cols).transpose(1,...  22.5 us
    slice x44, local copies, waits for them, and re-layouts, body(): lax.associative_scan(merge_state, (jnp.exp(log_decay), drive), axis=1)  11.2 us
    pad x24, local copies, waits for them, and re-layouts, body(): lax.associative_scan(merge_state, (jnp.exp(log_decay), drive), axis=1)  10.2 us
  transfers between devices with their start and end apart: 5, of which 2 were waited for; matrix products, arithmetic and copies ran while one was open for 24% of the time, Pallas kernels for 0%

commit v1 on v0

--- a/solution.py
+++ b/solution.py
@@ -109,7 +109,14 @@
         jnp.zeros((seq_count, kv_local, head_group * seq_span), jnp.float32),
         jnp.zeros((seq_count, kv_local, head_group * seq_span, head_dim), jnp.float32),
     )
-    shard_part = lax.all_gather(key_value, "sp", axis=1, tiled=True)
+    n_dev = lax.axis_size("sp")
+    hops = [(i, (i + 1) % n_dev) for i in range(n_dev)]
+    parts = [key_value]
+    for far in range(1, n_dev):
+        parts = [lax.ppermute(parts[0], "sp", hops), *parts]
+    out = jnp.concatenate(parts, axis=1)
+    shift = (lax.axis_index("sp") + 1) * parts[-1].shape[1]
+    shard_part = jnp.roll(out, shift, axis=1)
     offset = jnp.int32(0)
     length = shard_part.shape[1]
     sub_size = block_length(length, seq_span)

time: 265 us -> 375 us (1.42)
  local copies, waits for them, and re-layouts: 35.4 us -> 107 us
  waiting for transfers between devices: 25.4 us -> 70.1 us
  blocking collectives: 147 us -> 116 us
  other arithmetic: 24.8 us -> 40.3 us
  matrix products: 14.1 us -> 19.7 us
    ppermute x0 -> x7, waiting for transfers between devices: none -> 46.5 us  [body(): parts = [lax.ppermute(parts[0], 'sp', hops), *parts]]
    slice x44, local copies, waits for them, and re-layouts: 11.2 us -> 51.4 us  [body(): lax.associative_scan(merge_state, (jnp.exp(log_decay), drive), axis=1)]
    all_gather x1 -> x0, blocking collectives: 29.7 us -> none  [body(): shard_part = lax.all_gather(key_value, 'sp', axis=1, tiled=True)]
    unnamed x33 -> x58, local copies, waits for them, and re-layouts: 0.72 us -> 22.8 us
    sub x0 -> x2, local copies, waits for them, and re-layouts: none -> 9.44 us  [work(): scores.reshape(seq_count, kv_local, head_group, seq_span, sub_size)]
    add x13, other arithmetic: 4.34 us -> 13.7 us  [merge_state(): return (earlier[0] * later[0], later[0] * earlier[1] + later[1])]
    concatenate x11, other arithmetic: 3.16 us -> 7.83 us  [body(): lax.associative_scan(merge_state, (jnp.exp(log_decay), drive), axis=1)]
  transfers between devices with their start and end apart: 5 -> 12, of which waited for: 2 -> 8; matrix products, arithmetic and copies ran while one was open for 24% -> 42% of each run, Pallas kernels for 0% -> 0%
where the time goes in v1:
time: 375 us; the launch traced here: 371 us
  blocking collectives  116 us (31%)
  local copies, waits for them, and re-layouts  107 us (29%)
  waiting for transfers between devices  70.1 us (19%)
  other arithmetic  40.3 us (11%)
  matrix products  19.7 us (5%)
  between operations  13.9 us (4%)
    slice x44, local copies, waits for them, and re-layouts, body(): lax.associative_scan(merge_state, (jnp.exp(log_decay), drive), axis=1)  51.4 us
    ppermute x7, waiting for transfers between devices, body(): parts = [lax.ppermute(parts[0], 'sp', hops), *parts]  46.5 us
    all_gather x1, blocking collectives, body(): lax.all_gather(value_weight, 'sp', axis=0, tiled=True)  33.1 us
    all_gather x1, blocking collectives, body(): lax.all_gather(key_weight, 'sp', axis=0, tiled=True)  31 us
    all_gather x1, blocking collectives, body(): lax.all_gather(cum_decay[:, seq_span - 1][None], 'sp', axis=0, tiled=True)  26.1 us
    all_gather x1, blocking collectives, body(): lax.all_gather(local_state[:, seq_span - 1][None], 'sp', axis=0, tiled=True)  26.1 us
    unnamed x58, local copies, waits for them, and re-layouts  22.8 us
    reduce_scatter x1, waiting for transfers between devices, body(): lax.psum_scatter(terms.reshape(row_count, pieces, out_cols).transpose(1,...  22.1 us
  transfers between devices with their start and end apart: 12, of which 8 were waited for; matrix products, arithmetic and copies ran while one was open for 42% of the time, Pallas kernels for 0%

profile of v1, /device:TPU:0, one launch (start us, length us, event | category | flops | bytes accessed | tf_op | source)
XLA Modules:
  0.0 370.7 jit_solution(11870754059117342559)
XLA Ops:
  9.6 33.1 %all_gather.22 = bf16[2048,64]{0,1:T(8,128)(2,1)S(1)} all-gather(bf16[256,64]{0,1:T(8,128)(2,1)} %param.25), channel_id=1, replica_groups=mesh['sp'=8,'tp'=4] {'sp'}, dimensions={0}, use_global_device_ids=true | all-gather | bytes 294912 | tf_op jit(solution)/shard_map/all_gather | solution.py:77
  44.7 31.0 %all_gather.21 = bf16[2048,64]{0,1:T(8,128)(2,1)S(1)} all-gather(bf16[256,64]{0,1:T(8,128)(2,1)S(1)} %copy-done.12), channel_id=1, replica_groups=mesh['sp'=8,'tp'=4] {'sp'}, dimensions={0}, use_global_device_ids=true | all-gather | bytes 294912 | tf_op jit(solution)/shard_map/all_gather | solution.py:76
  77.9 5.5 %collective-permute-done = bf16[2,128,128]{1,2,0:T(8,128)(2,1)S(1)} collective-permute-done((bf16[2,128,128]{1,2,0:T(8,128)(2,1)S(1)}, bf16[2,128,128]{1,2,0:T(8,128)(2,1)S(1)}, u32[]{:S(2)}, u32[]{:S(2)}) %collective-permute-start) | collective-permute-done | bytes 65568 | tf_op jit(solution)/shard_map/ppermute | solution.py:116
  83.3 7.6 %collective-permute-done.1 = bf16[2,128,128]{1,2,0:T(8,128)(2,1)S(1)} collective-permute-done((bf16[2,128,128]{1,2,0:T(8,128)(2,1)S(1)}, bf16[2,128,128]{1,2,0:T(8,128)(2,1)S(1)}, u32[]{:S(2)}, u32[]{:S(2)}) %collective-permute-start.1) | collective-permute-done | bytes 65568 | tf_op jit(solution)/shard_map/ppermute | solution.py:116
  90.9 7.0 %collective-permute-done.2 = bf16[2,128,128]{1,2,0:T(8,128)(2,1)S(1)} collective-permute-done((bf16[2,128,128]{1,2,0:T(8,128)(2,1)S(1)}, bf16[2,128,128]{1,2,0:T(8,128)(2,1)S(1)}, u32[]{:S(2)}, u32[]{:S(2)}) %collective-permute-start.2) | collective-permute-done | bytes 65568 | tf_op jit(solution)/shard_map/ppermute | solution.py:116
  98.0 6.9 %collective-permute-done.3 = bf16[2,128,128]{1,2,0:T(8,128)(2,1)S(1)} collective-permute-done((bf16[2,128,128]{1,2,0:T(8,128)(2,1)S(1)}, bf16[2,128,128]{1,2,0:T(8,128)(2,1)S(1)}, u32[]{:S(2)}, u32[]{:S(2)}) %collective-permute-start.3) | collective-permute-done | bytes 65568 | tf_op jit(solution)/shard_map/ppermute | solution.py:116
  106.2 5.8 %collective-permute-done.4 = bf16[2,128,128]{1,2,0:T(8,128)(2,1)S(1)} collective-permute-done((bf16[2,128,128]{1,2,0:T(8,128)(2,1)S(1)}, bf16[2,128,128]{1,2,0:T(8,128)(2,1)S(1)}, u32[]{:S(2)}, u32[]{:S(2)}) %collective-permute-start.4) | collective-permute-done | bytes 65568 | tf_op jit(solution)/shard_map/ppermute | solution.py:116
  113.2 6.7 %collective-permute-done.5 = bf16[2,128,128]{1,2,0:T(8,128)(2,1)} collective-permute-done((bf16[2,128,128]{1,2,0:T(8,128)(2,1)S(1)}, bf16[2,128,128]{1,2,0:T(8,128)(2,1)}, u32[]{:S(2)}, u32[]{:S(2)}) %collective-permute-start.5) | collective-permute-done | bytes 65568 | tf_op jit(solution)/shard_map/ppermute | solution.py:116
  119.9 7.2 %collective-permute-done.6 = bf16[2,128,128]{1,2,0:T(8,128)(2,1)} collective-permute-done((bf16[2,128,128]{1,2,0:T(8,128)(2,1)}, bf16[2,128,128]{1,2,0:T(8,128)(2,1)}, u32[]{:S(2)}, u32[]{:S(2)}) %collective-permute-start.6) | collective-permute-done | bytes 65568 | tf_op jit(solution)/shard_map/ppermute | solution.py:116
  150.6 2.3 copy.58
  154.9 22.4 %conditional.1 = ((f32[2,1,512]{2,0,1:T(2,128)S(1)}, f32[2,1,512,64]{2,3,0,1:T(8,128)S(1)})) conditional(s32[]{:T(128)} %convert_element_type.126, (f32[2,1,512]{2,0,1:T(2,128)S(1)}, f32[2,1,512,64]{2,3,0,1:T(8,128)S(1)}) %tuple.45, (s32[]{:T(128)}, s32[4,128]{1,0:T(4,128)S(1)}, s32[]{:T(128)}, s32[]{:T(128)}, bf16[2,2048,128]{1,2,0:T(8,128)(2,1)}, ...), branch_computations={%region_3.4_spmd, %region_4.0_spmd.clone} | conditional | flops 278534656 | bytes 50899244 | solution.py:165
  158.0 3.9 %sub.86 = f32[2,4,128,1024]{2,1,3,0:T(4,128)} broadcast(f32[2,4,1024]{1,2,0:T(8,128)S(1)} %copy.54), dimensions={0,1,3} | broadcast | bytes 4227072 | tf_op jit(solution)/shard_map/while/body/eval_jaxpr/cond/branch_1_fun/sub | solution.py:143
  161.9 5.5 %sub.87 = f32[2,512,1024]{1,2,0:T(8,128)} reshape(f32[2,4,128,1024]{2,1,3,0:T(4,128)} %sub.86) | data formatting | bytes 8388608 | tf_op jit(solution)/shard_map/while/body/eval_jaxpr/cond/branch_1_fun/sub | solution.py:143
  167.5 5.6 %fusion.77 = (f32[2,512]{1,0:T(2,128)S(1)}, f32[2,512,1024]{1,2,0:T(8,128)}) fusion(f32[2,512,1024]{1,2,0:T(8,128)} %sub.87, f32[2,512]{1,0:T(2,128)S(1)} %bitcast.187, bf16[2,512,64]{1,2,0:T(8,128)(2,1)S(1)} %reshape.387, bf16[2,2048,128]{1,2,0:T(8,128)(2,1)} %get-tuple-element.267, s32[]{:T(128)S(6)} %select_n.104, pred[512,1024]{0,1:T(8,128)(4,1)S(1)} %copy-done.4), kind=kOutput, calls=%fused_computation.186 | convolution fusion | flops 139459584 | bytes 9314308 | tf_op jit(solution)/shard_map/while/body/eval_jaxpr/cond/branch_1_fun/bhqd,bkhd->bhqk/dot_general | solution.py:137
  173.1 3.2 fusion.9
  187.1 2.0 convert_multiply_fusion
  264.8 2.1 pad.129
  270.9 2.3 pad.118
  275.6 2.3 pad.132
  279.3 26.1 %all-gather = f32[16,1,256]{2,1,0:T(1,128)S(1)} all-gather(f32[2,1,256]{2,1,0:T(1,128)S(1)} %slice_add_fusion.4), channel_id=2, replica_groups=mesh['sp'=8,'tp'=4] {'sp'}, dimensions={0}, use_global_device_ids=true | all-gather | bytes 18432 | tf_op jit(solution)/shard_map/all_gather | solution.py:206
  305.4 26.1 %all-gather.1 = f32[16,1,256]{2,1,0:T(1,128)S(1)} all-gather(f32[2,1,256]{2,1,0:T(1,128)S(1)} %slice_add_fusion.3), channel_id=3, replica_groups=mesh['sp'=8,'tp'=4] {'sp'}, dimensions={0}, use_global_device_ids=true | all-gather | bytes 18432 | tf_op jit(solution)/shard_map/all_gather | solution.py:205
  332.0 3.0 fusion.82
  335.0 1.8 copy.71
  342.0 22.1 %reduce-scatter.2.cloned.1.call-done = bf16[256,512]{1,0:T(8,128)(2,1)} async-done(((bf16[1024,512]{1,0:T(8,128)(2,1)}), bf16[256,512]{1,0:T(8,128)(2,1)}) %reduce-scatter.2.cloned.1.call-update) | async-done | bytes 262160 | tf_op jit(solution)/shard_map/reduce_scatter | solution.py:228
  (260 shorter events, 137.8 us)
Async XLA Ops:
  6.5 175.3 %copy-start = (bf16[256,2048]{1,0:T(8,128)(2,1)S(1)}, bf16[256,2048]{1,0:T(8,128)(2,1)}, u32[]{:S(2)}) copy-start(bf16[256,2048]{1,0:T(8,128)(2,1)} %param.38) | copy-start | bytes 3145732
  6.5 98.3 %copy-start.2 = (bf16[2,128,2048]{2,1,0:T(8,128)(2,1)S(1)}, bf16[2,128,2048]{2,1,0:T(8,128)(2,1)}, u32[]{:S(2)}) copy-start(bf16[2,128,2048]{2,1,0:T(8,128)(2,1)} %param.21) | copy-start | bytes 3145732
  6.5 98.3 %copy-start.11 = (f32[2048]{0:T(1024)S(1)}, f32[2048]{0:T(1024)}, u32[]{:S(2)}) copy-start(f32[2048]{0:T(1024)} %param.22) | copy-start | bytes 24580
  6.5 38.2 %copy-start.12 = (bf16[256,64]{0,1:T(8,128)(2,1)S(1)}, bf16[256,64]{0,1:T(8,128)(2,1)}, u32[]{:S(2)}) copy-start(bf16[256,64]{0,1:T(8,128)(2,1)} %param.24) | copy-start | bytes 98308
  6.5 69.6 %copy-start.16 = (f32[64]{0:T(128)S(1)}, f32[64]{0:T(128)}, u32[]{:S(2)}) copy-start(f32[64]{0:T(128)} %param.27) | copy-start | bytes 772
  6.5 144.1 %all-gather.6.cloned.1.call-start = ((), (), s32[]{:S(2)}) async-start(), calls=%async_computation.1 | async-start | bytes 1179648 | tf_op jit(solution)/shard_map/all_gather | solution.py:75
  7.3 170.5 %all-gather.8.cloned.1.call-start = ((), (), s32[]{:S(2)}) async-start(), calls=%async_computation.2 | async-start | bytes 1179648 | tf_op jit(solution)/shard_map/all_gather | solution.py:78
  8.0 323.9 %all-gather.10.cloned.1.call-start = ((), (), s32[]{:S(2)}) async-start(), calls=%async_computation.3 | async-start | bytes 1179648 | tf_op jit(solution)/shard_map/all_gather | solution.py:79
  9.6 103.0 %copy-start.15 = (bf16[4,256]{1,0:T(4,128)(2,1)S(1)}, bf16[4,256]{1,0:T(4,128)(2,1)}, u32[]{:S(2)}) copy-start(bf16[4,256]{1,0:T(4,128)(2,1)} %param.31) | copy-start | bytes 6148
  9.6 110.2 %copy-start.20 = (f32[256]{0:T(256)S(1)}, f32[256]{0:T(256)}, u32[]{:S(2)}) copy-start(f32[256]{0:T(256)} %param.34) | copy-start | bytes 3076
  76.2 7.1 %collective-permute-start = (bf16[2,128,128]{1,2,0:T(8,128)(2,1)S(1)}, bf16[2,128,128]{1,2,0:T(8,128)(2,1)S(1)}, u32[]{:S(2)}, u32[]{:S(2)}) collective-permute-start(bf16[2,128,128]{1,2,0:T(8,128)(2,1)S(1)} %pad_maximum_fusion.3), channel_id=1, source_target_pairs={{0,4},{4,8},{8,12},{12,16},{16,20},{20,24},{24,28},{28,0},{1,5},{5... | collective-permute-start | bytes 196616 | tf_op jit(solution)/shard_map/ppermute | solution.py:116
  83.3 36.5 %copy-start.5 = (bf16[2,128,128]{1,2,0:T(8,128)(2,1)}, bf16[2,128,128]{1,2,0:T(8,128)(2,1)S(1)}, u32[]{:S(2)}) copy-start(bf16[2,128,128]{1,2,0:T(8,128)(2,1)S(1)} %collective-permute-done) | copy-start | bytes 196612
  83.3 7.6 %collective-permute-start.1 = (bf16[2,128,128]{1,2,0:T(8,128)(2,1)S(1)}, bf16[2,128,128]{1,2,0:T(8,128)(2,1)S(1)}, u32[]{:S(2)}, u32[]{:S(2)}) collective-permute-start(bf16[2,128,128]{1,2,0:T(8,128)(2,1)S(1)} %collective-permute-done), channel_id=1, source_target_pairs={{0,4},{4,8},{8,12},{12,16},{16,20},{20,24},{24,28},{28,0},{1,5},{5... | collective-permute-start | bytes 196616 | tf_op jit(solution)/shard_map/ppermute | solution.py:116
  90.9 29.0 %copy-start.6 = (bf16[2,128,128]{1,2,0:T(8,128)(2,1)}, bf16[2,128,128]{1,2,0:T(8,128)(2,1)S(1)}, u32[]{:S(2)}) copy-start(bf16[2,128,128]{1,2,0:T(8,128)(2,1)S(1)} %collective-permute-done.1) | copy-start | bytes 196612
  90.9 7.0 %collective-permute-start.2 = (bf16[2,128,128]{1,2,0:T(8,128)(2,1)S(1)}, bf16[2,128,128]{1,2,0:T(8,128)(2,1)S(1)}, u32[]{:S(2)}, u32[]{:S(2)}) collective-permute-start(bf16[2,128,128]{1,2,0:T(8,128)(2,1)S(1)} %collective-permute-done.1), channel_id=1, source_target_pairs={{0,4},{4,8},{8,12},{12,16},{16,20},{20,24},{24,28},{28,0},{1,5},{5... | collective-permute-start | bytes 196616 | tf_op jit(solution)/shard_map/ppermute | solution.py:116
  97.9 7.0 %collective-permute-start.3 = (bf16[2,128,128]{1,2,0:T(8,128)(2,1)S(1)}, bf16[2,128,128]{1,2,0:T(8,128)(2,1)S(1)}, u32[]{:S(2)}, u32[]{:S(2)}) collective-permute-start(bf16[2,128,128]{1,2,0:T(8,128)(2,1)S(1)} %collective-permute-done.2), channel_id=1, source_target_pairs={{0,4},{4,8},{8,12},{12,16},{16,20},{20,24},{24,28},{28,0},{1,5},{5... | collective-permute-start | bytes 196616 | tf_op jit(solution)/shard_map/ppermute | solution.py:116
  97.9 266.2 %reduce-scatter.2.cloned.1.call-start = ((), (), s32[]{:S(2)}) async-start(), calls=%async_computation.4 | async-start | bytes 1310720 | tf_op jit(solution)/shard_map/reduce_scatter | solution.py:228
  104.9 7.1 %collective-permute-start.4 = (bf16[2,128,128]{1,2,0:T(8,128)(2,1)S(1)}, bf16[2,128,128]{1,2,0:T(8,128)(2,1)S(1)}, u32[]{:S(2)}, u32[]{:S(2)}) collective-permute-start(bf16[2,128,128]{1,2,0:T(8,128)(2,1)S(1)} %collective-permute-done.3), channel_id=1, source_target_pairs={{0,4},{4,8},{8,12},{12,16},{16,20},{20,24},{24,28},{28,0},{1,5},{5... | collective-permute-start | bytes 196616 | tf_op jit(solution)/shard_map/ppermute | solution.py:116
  106.2 46.7 %copy-start.3 = (bf16[2,128,2048]{2,1,0:T(8,128)(2,1)S(1)}, bf16[2,128,2048]{2,1,0:T(8,128)(2,1)}, u32[]{:S(2)}) copy-start(bf16[2,128,2048]{2,1,0:T(8,128)(2,1)} %multiply_convert_fusion) | copy-start | bytes 3145732
  106.2 48.4 %copy-start.21 = (f32[64]{0:T(128)S(1)}, f32[64]{0:T(128)}, u32[]{:S(2)}) copy-start(f32[64]{0:T(128)} %param.26) | copy-start | bytes 772
  112.5 7.3 %collective-permute-start.5 = (bf16[2,128,128]{1,2,0:T(8,128)(2,1)S(1)}, bf16[2,128,128]{1,2,0:T(8,128)(2,1)}, u32[]{:S(2)}, u32[]{:S(2)}) collective-permute-start(bf16[2,128,128]{1,2,0:T(8,128)(2,1)S(1)} %collective-permute-done.4), channel_id=1, source_target_pairs={{0,4},{4,8},{8,12},{12,16},{16,20},{20,24},{24,28},{28,0},{1,5},{5... | collective-permute-start | bytes 196616 | tf_op jit(solution)/shard_map/ppermute | solution.py:116
  119.8 7.3 %collective-permute-start.6 = (bf16[2,128,128]{1,2,0:T(8,128)(2,1)}, bf16[2,128,128]{1,2,0:T(8,128)(2,1)}, u32[]{:S(2)}, u32[]{:S(2)}) collective-permute-start(bf16[2,128,128]{1,2,0:T(8,128)(2,1)} %collective-permute-done.5), channel_id=1, source_target_pairs={{0,4},{4,8},{8,12},{12,16},{16,20},{20,24},{24,28},{28,0},{1,5},{5... | collective-permute-start | bytes 196616 | tf_op jit(solution)/shard_map/ppermute | solution.py:116
  179.5 2.8 collective-permute-start.7
  270.8 68.3 %copy-start.19 = (f32[256]{0:T(256)S(1)}, f32[256]{0:T(256)}, u32[]{:S(2)}) copy-start(f32[256]{0:T(256)} %param.37) | copy-start | bytes 3076
  (11 other events, 96.6 us)
Sparse Core Ops, SparseCore 0:
  9.5 43.5 all-gather.5
  55.2 40.4 all-gather.7
  98.0 41.9 all-gather.9
  342.1 21.9 reduce-scatter.1
